TPU v7x, 32 devices: a whole 2x2x4 slice. The times are simulated.
32 devices in a mesh: dp: 4 (over y, x), kv: 4 (over z), tp: 2 (over core).
Axes of the slice: x: 2, y: 2, z: 4, core: 2. Of those that a mesh axis runs over, the one named last changes fastest.
Arguments:
- tokens: bfloat16 [8192, 2048], P(('dp', 'kv')), parts along dimension 0, may hold values from -60 to 60, as said below
- chosen: int32 [128, 16], P(('dp', 'kv')), parts along dimension 0, may hold values from -1 to 31, as said below
- query_weight: bfloat16 [2048, 1024], P('kv', 'tp'), may hold values from -0.125 to 0.125
- key_matrix: bfloat16 [2048, 128], P('kv', 'tp'), may hold values from -0.125 to 0.125
- value_matrix: bfloat16 [2048, 128], P('kv', 'tp'), may hold values from -0.125 to 0.125
- out_weight: bfloat16 [1024, 2048], P('tp', 'kv'), may hold values from -0.1875 to 0.1875
- out_gain: float32 [2048], replicated, may hold values from 0.1 to 1.9
Outputs:
- mixed_out: bfloat16 [8192, 2048], P(('dp', 'kv', 'tp')), parts along dimension 0
There are 4 independent parts, one for each index of `dp`. A program takes and returns all parts, laid end to end along the dimension named above; an argument that names none is the same for every part. Nothing has to cross between parts.
Inputs may be any that keep to these rules, and one draw needn't show every extreme that they name: tokens are of order one apart from few rows. chosen[g, 0] = g; every other entry of row g is -1 or a block below g, and the entries of a row other than -1 are distinct; the blocks that the rows of one device name on any single other device are at most 2 different ones, and this is reached.
All inputs are finite; a program needn't handle non-finite values.
Results may differ from a plain program's by a relative error of at most 0.012.
The roundings to bfloat16 on the way count: a program that leaves them out, or rounds other values in their place, can miss the bound.
Values may be sent and summed in bfloat16 or wider, within the bound.
A program may use at most 64 MiB of HBM per device.

v0:
```python
import jax
import jax.numpy as jnp
from jax import lax
from jax.sharding import PartitionSpec as P

HEAD_WIDTH = 64
BLOCK_LENGTH = 64


def per_device(tokens, chosen, query_weight, key_matrix, value_matrix, out_weight, out_gain):
    tok_rows = tokens.shape[0]
    blocks = tok_rows // BLOCK_LENGTH
    device = lax.axis_index("kv")
    kv_count = lax.axis_size("kv")
    whole_query, whole_key, whole_value = (
        lax.all_gather(query_weight, "kv", axis=0, tiled=True),
        lax.all_gather(key_matrix, "kv", axis=0, tiled=True),
        lax.all_gather(value_matrix, "kv", axis=0, tiled=True),
    )
    query_rows = jnp.dot(tokens, whole_query, preferred_element_type=jnp.float32).astype(
        jnp.bfloat16
    )
    key_rows = jnp.dot(tokens, whole_key, preferred_element_type=jnp.float32).astype(jnp.bfloat16)
    value_rows = jnp.dot(tokens, whole_value, preferred_element_type=jnp.float32).astype(
        jnp.bfloat16
    )
    paired = jnp.concatenate([key_rows, value_rows], axis=1)
    pair_width = paired.shape[1]
    safe_ids = jnp.maximum(chosen, 0)
    everyone = lax.all_gather(paired, "kv", axis=0, tiled=True).reshape(
        kv_count * blocks, BLOCK_LENGTH, pair_width
    )
    picked = jnp.take(everyone, safe_ids, axis=0)
    head_count = query_rows.shape[1] // HEAD_WIDTH
    grouped = query_rows.reshape(blocks, BLOCK_LENGTH, head_count, HEAD_WIDTH)
    offsets = jnp.arange(BLOCK_LENGTH, dtype=jnp.int32)
    query_pos = (device * blocks + jnp.arange(blocks, dtype=jnp.int32))[
        :, None
    ] * BLOCK_LENGTH + offsets[None, :]
    key_pos = safe_ids[:, :, None] * BLOCK_LENGTH + offsets[None, None, :]
    visible = (chosen >= 0)[:, None, :, None] & (
        key_pos[:, None, :, :] <= query_pos[:, :, None, None]
    )

    def attend_block(inputs):
        query_block, pair_block, seen = inputs
        block_keys = pair_block[..., :HEAD_WIDTH]
        block_values = pair_block[..., HEAD_WIDTH:]
        scores = jnp.einsum(
            "qgd,skd->gqsk", query_block, block_keys, preferred_element_type=jnp.float32
        ) * HEAD_WIDTH ** (-0.5)
        scores = jnp.where(seen[None], scores, -1e30)
        row_max = jnp.max(scores, axis=(2, 3), keepdims=True)
        expon = jnp.exp(scores - row_max)
        row_sum = jnp.sum(expon, axis=(2, 3), keepdims=True)
        weights_bf = (expon / row_sum).astype(jnp.bfloat16)
        result = jnp.einsum(
            "gqsk,skd->qgd", weights_bf, block_values, preferred_element_type=jnp.float32
        )
        return result.astype(jnp.bfloat16)

    attended = lax.map(attend_block, (grouped, picked, visible))
    attended = attended.reshape(tok_rows, head_count * HEAD_WIDTH)
    whole_out = lax.all_gather(out_weight, "kv", axis=1, tiled=True)
    mixed = lax.psum_scatter(
        jnp.dot(attended, whole_out, preferred_element_type=jnp.float32).astype(jnp.bfloat16),
        "tp",
        scatter_dimension=0,
        tiled=True,
    ).astype(jnp.float32)
    normed = mixed * lax.rsqrt(jnp.mean(mixed * mixed, axis=-1, keepdims=True) + 1e-06) * out_gain
    return normed.astype(jnp.bfloat16)


def solution(mesh):
    placed = (
        P(("dp", "kv"), None),
        P(("dp", "kv"), None),
        P("kv", "tp"),
        P("kv", "tp"),
        P("kv", "tp"),
        P("tp", "kv"),
        P(),
    )
    return jax.shard_map(
        per_device,
        mesh=mesh,
        in_specs=placed,
        out_specs=P(("dp", "kv", "tp"), None),
        check_vma=False,
    )
```

profile of v0, /device:TPU:0, one launch (start us, length us, event | category | flops | bytes accessed | tf_op | source)
XLA Modules:
  0.0 154.0 jit_solution(18030068477290165004)
XLA Ops:
  9.5 16.8 %all_gather.16 = bf16[2048,64]{0,1:T(8,128)(2,1)S(1)} all-gather(bf16[512,64]{0,1:T(8,128)(2,1)} %param.13), channel_id=1, replica_groups=mesh['dp'=4,'kv'=4,'tp'=2] {'kv'}, dimensions={0}, use_global_device_ids=true | all-gather | bytes 327680 | tf_op jit(solution)/shard_map/all_gather | solution.py:18
  26.4 17.1 %all_gather.15 = bf16[2048,64]{0,1:T(8,128)(2,1)S(1)} all-gather(bf16[512,64]{0,1:T(8,128)(2,1)} %param.12), channel_id=1, replica_groups=mesh['dp'=4,'kv'=4,'tp'=2] {'kv'}, dimensions={0}, use_global_device_ids=true | all-gather | bytes 327680 | tf_op jit(solution)/shard_map/all_gather | solution.py:17
  45.1 22.0 %all_gather.17 = bf16[2048,128]{0,1:T(8,128)(2,1)S(1)} all-gather(bf16[512,128]{0,1:T(8,128)(2,1)S(1)} %pad_maximum_fusion), channel_id=1, replica_groups=mesh['dp'=4,'kv'=4,'tp'=2] {'kv'}, dimensions={0}, use_global_device_ids=true | all-gather | bytes 655360 | tf_op jit(solution)/shard_map/all_gather | solution.py:30
  67.6 2.2 %gather_fusion = bf16[128,64,128]{2,1,0:T(8,128)(2,1)} fusion(bf16[32,64,128]{2,1,0:T(8,128)(2,1)S(1)} %bitcast.82, s32[1024]{0:T(1024)S(1)} %pad_clamp_fusion), kind=kCustom, calls=%fused_computation | custom fusion | bytes 4194816 | tf_op jit(solution)/shard_map/jit(_take)/gather | solution.py:33
  69.7 3.2 %broadcast_select_fusion = bf16[8,16,64,128]{3,2,1,0:T(8,128)(2,1)} fusion(bf16[8,16,64,128]{3,2,1,0:T(8,128)(2,1)} %bitcast.83, pred[8,16]{1,0:T(8,128)(4,1)S(1)} %get-tuple-element.56), kind=kLoop, calls=%fused_computation.27 | loop fusion | flops 1048576 | bytes 4194432 | tf_op jit(solution)/shard_map/jit(_take)/select_n | solution.py:33
  72.9 1.5 compare_and_fusion
  74.5 3.6 %convolution_convert_fusion.1 = bf16[512,512]{1,0:T(8,128)(2,1)} fusion(bf16[512,2048]{1,0:T(8,128)(2,1)S(1)} %copy-done, bf16[2048,512]{1,0:T(8,128)(2,1)} %all-gather.3.cloned.1.call-done), kind=kOutput, calls=%fused_computation.28 | convolution fusion | flops 1074003968 | bytes 4718592 | tf_op jit(solution)/shard_map/dot_general | solution.py:20
  78.1 2.4 %reshape.58 = bf16[8,64,8,64]{3,2,1,0:T(8,128)(2,1)} reshape(bf16[512,512]{1,0:T(8,128)(2,1)} %convolution_convert_fusion.1) | data formatting | bytes 1048576 | tf_op jit(solution)/shard_map/reshape | solution.py:35
  80.5 47.3 %while.10 = (s32[]{:T(128)}, bf16[8,64,8,64]{3,2,1,0:T(8,128)(2,1)}, bf16[8,16,64,128]{3,2,1,0:T(8,128)(2,1)}, pred[8,64,16,64]{1,3,2,0:T(8,128)(4,1)S(1)}, bf16[8,64,8,64]{3,2,1,0:T(8,128)(2,1)}, /*index=5*/s32[]{:T(128)}) while((s32[]{:T(128)}, bf16[8,64,8,64]{3,2,1,0:T(8,128)(2,1)}, bf16[8,16,64,128]{3,2,1,0:T(8,128)(2,1)}, ...), condition=%wide.region_3.4_spmd, body=%wide.region_0.3_spmd.sunk | while | flops 140540928 | bytes 8268369 | solution.py:62
  83.3 1.0 fusion.24
  84.3 1.2 fusion.25
  90.2 1.2 fusion.25
  96.2 1.2 fusion.25
  102.1 1.2 fusion.25
  108.0 1.2 fusion.25
  113.9 1.2 fusion.25
  119.8 1.2 fusion.25
  124.7 1.0 fusion.24
  125.7 1.2 fusion.25
  127.8 1.9 %reshape.59 = bf16[512,512]{1,0:T(8,128)(2,1)S(1)} reshape(bf16[8,64,8,64]{3,2,1,0:T(8,128)(2,1)} %get-tuple-element.32) | data formatting | bytes 1048576 | tf_op jit(solution)/shard_map/reshape | solution.py:63
  129.7 4.2 %convolution_convert_fusion = bf16[512,2048]{1,0:T(8,128)(2,1)} fusion(bf16[512,512]{1,0:T(8,128)(2,1)S(1)} %reshape.59, bf16[512,2048]{1,0:T(8,128)(2,1)} %all-gather.5.cloned.1.call-done), kind=kOutput, calls=%fused_computation.21 | convolution fusion | flops 1074790400 | bytes 4718592 | tf_op jit(solution)/shard_map/dot_general | solution.py:66
  133.9 9.6 %reduce-scatter.2.cloned.1.call-done = bf16[256,2048]{1,0:T(8,128)(2,1)} async-done(((bf16[512,2048]{1,0:T(8,128)(2,1)}), bf16[256,2048]{1,0:T(8,128)(2,1)}) %reduce-scatter.2.cloned.1.call-update) | async-done | bytes 1048592 | tf_op jit(solution)/shard_map/reduce_scatter | solution.py:65
  143.5 1.5 fusion.9
  145.0 2.5 %fusion.11 = bf16[256,2048]{1,0:T(8,128)(2,1)} fusion(bf16[256,2048]{1,0:T(8,128)(2,1)} %reduce-scatter.2.cloned.1.call-done, f32[2048]{0:T(1024)S(1)} %copy-done.1, f32[256]{0:T(256)S(1)} %add_rsqrt_fusion), kind=kLoop, calls=%fused_computation.26 | loop fusion | flops 2097152 | bytes 2106368 | tf_op jit(solution)/shard_map/convert_element_type | solution.py:72
  (79 shorter events, 40.0 us)
Async XLA Ops:
  6.5 37.0 %copy-start = (bf16[512,2048]{1,0:T(8,128)(2,1)S(1)}, bf16[512,2048]{1,0:T(8,128)(2,1)}, u32[]{:S(2)}) copy-start(bf16[512,2048]{1,0:T(8,128)(2,1)} %param.9) | copy-start | bytes 6291460
  6.5 67.9 %all-gather.3.cloned.1.call-start = ((), (), s32[]{:S(2)}) async-start(), calls=%async_computation.1 | async-start | bytes 2621440 | tf_op jit(solution)/shard_map/all_gather | solution.py:16
  7.3 122.4 %all-gather.5.cloned.1.call-start = ((), (), s32[]{:S(2)}) async-start(), calls=%async_computation.2 | async-start | bytes 2621440 | tf_op jit(solution)/shard_map/all_gather | solution.py:64
  8.0 135.5 %reduce-scatter.2.cloned.1.call-start = ((), (), s32[]{:S(2)}) async-start(), calls=%async_computation.3 | async-start | bytes 3145728 | tf_op jit(solution)/shard_map/reduce_scatter | solution.py:65
  133.8 11.2 %copy-start.1 = (f32[2048]{0:T(1024)S(1)}, f32[2048]{0:T(1024)}, u32[]{:S(2)}) copy-start(f32[2048]{0:T(1024)} %param.15) | copy-start | bytes 24580
Sparse Core Ops, SparseCore 0:
  8.9 61.9 all-gather.2
  72.5 44.4 all-gather.4
  134.0 9.4 reduce-scatter.1
where the time goes:
time: 155 us; the launch traced here: 154 us
  blocking collectives  56 us (36%)
  local copies, waits for them, and re-layouts  28.5 us (18%)
  matrix products  26.5 us (17%)
  other arithmetic  18.5 us (12%)
  between operations  13.2 us (9%)
  waiting for transfers between devices  11.1 us (7%)
    all_gather x1, blocking collectives, per_device(): lax.all_gather(paired, 'kv', axis=0, tiled=True)  22 us
    all_gather x1, blocking collectives, per_device(): lax.all_gather(key_matrix, 'kv', axis=0, tiled=True)  17.1 us
    all_gather x1, blocking collectives, per_device(): lax.all_gather(value_matrix, 'kv', axis=0, tiled=True)  16.8 us
    dot_general x8, matrix products, attend_block(): jnp.einsum('gqsk,skd->qgd', weights_bf, block_values, preferred_element_t...  9.99 us
    reduce_scatter x1, waiting for transfers between devices, per_device(): lax.psum_scatter(jnp.dot(attended, whole_out, preferred_element_type=jnp....  9.61 us
    reduce_sum x8, other arithmetic, attend_block(): row_sum = jnp.sum(expon, axis=(2, 3), keepdims=True)  8.16 us
    squeeze x8, local copies, waits for them, and re-layouts, per_device(): attended = lax.map(attend_block, (grouped, picked, visible))  7.8 us
    dynamic_slice x8, local copies, waits for them, and re-layouts, per_device(): attended = lax.map(attend_block, (grouped, picked, visible))  7.37 us
  transfers between devices with their start and end apart: 3, of which 1 were waited for; matrix products, arithmetic and copies ran while one was open for 42% of the time, Pallas kernels for 0%

commit v1 on v0

--- a/solution.py
+++ b/solution.py
@@ -5,6 +5,19 @@
 
 HEAD_WIDTH = 64
 BLOCK_LENGTH = 64
+
+
+def collect(shard, axis, dim):
+    peers, mine, span = (lax.axis_size(axis), lax.axis_index(axis), shard.shape[dim])
+    forward = [(i, (i + 1) % peers) for i in range(peers)]
+    out = jnp.zeros((*shard.shape[:dim], peers * span, *shard.shape[dim + 1 :]), shard.dtype)
+    held = shard
+    for hop in range(peers):
+        owner = (mine - hop) % peers
+        out = lax.dynamic_update_slice_in_dim(out, held, owner * span, axis=dim)
+        if hop < peers - 1:
+            held = lax.ppermute(held, axis, forward)
+    return out
 
 
 def per_device(tokens, chosen, query_weight, key_matrix, value_matrix, out_weight, out_gain):
@@ -27,9 +40,7 @@
     paired = jnp.concatenate([key_rows, value_rows], axis=1)
     pair_width = paired.shape[1]
     safe_ids = jnp.maximum(chosen, 0)
-    everyone = lax.all_gather(paired, "kv", axis=0, tiled=True).reshape(
-        kv_count * blocks, BLOCK_LENGTH, pair_width
-    )
+    everyone = collect(paired, "kv", 0).reshape(kv_count * blocks, BLOCK_LENGTH, pair_width)
     picked = jnp.take(everyone, safe_ids, axis=0)
     head_count = query_rows.shape[1] // HEAD_WIDTH
     grouped = query_rows.reshape(blocks, BLOCK_LENGTH, head_count, HEAD_WIDTH)

time: 155 us -> 158 us (1.019)
  waiting for transfers between devices: 11.1 us -> 34.3 us
  blocking collectives: 56 us -> 34.3 us
  starting transfers between devices: 0.08 us -> 1.93 us
    ppermute x0 -> x3, waiting for transfers between devices: none -> 24 us  [collect(): held = lax.ppermute(held, axis, forward)]
    all_gather x1 -> x0, blocking collectives: 22 us -> none  [per_device(): lax.all_gather(paired, 'kv', axis=0, tiled=True)]
    broadcast_in_dim x8, local copies, waits for them, and re-layouts: 0.08 us -> 7.31 us  [attend_block(): scores = jnp.where(seen[None], scores, -1e+30)]
    dynamic_slice x8, local copies, waits for them, and re-layouts: 7.37 us -> 0.14 us  [per_device(): attended = lax.map(attend_block, (grouped, picked, visible))]
    ppermute x0 -> x3, starting transfers between devices: none -> 1.85 us  [collect(): held = lax.ppermute(held, axis, forward)]
  transfers between devices with their start and end apart: 3 -> 6, of which waited for: 1 -> 4; matrix products, arithmetic and copies ran while one was open for 42% -> 41% of each run, Pallas kernels for 0% -> 0%
where the time goes in v1:
time: 158 us; the launch traced here: 157 us
  waiting for transfers between devices  34.3 us (22%)
  blocking collectives  34.3 us (22%)
  local copies, waits for them, and re-layouts  28.2 us (18%)
  matrix products  26.5 us (17%)
  other arithmetic  18.3 us (12%)
  between operations  13.4 us (8%)
  starting transfers between devices  1.93 us (1%)
    ppermute x3, waiting for transfers between devices, collect(): held = lax.ppermute(held, axis, forward)  24 us
    all_gather x1, blocking collectives, per_device(): lax.all_gather(key_matrix, 'kv', axis=0, tiled=True)  17.7 us
    all_gather x1, blocking collectives, per_device(): lax.all_gather(value_matrix, 'kv', axis=0, tiled=True)  16.7 us
    dot_general x8, matrix products, attend_block(): jnp.einsum('gqsk,skd->qgd', weights_bf, block_values, preferred_element_t...  9.99 us
    reduce_scatter x1, waiting for transfers between devices, per_device(): lax.psum_scatter(jnp.dot(attended, whole_out, preferred_element_type=jnp....  9.47 us
    reduce_sum x8, other arithmetic, attend_block(): row_sum = jnp.sum(expon, axis=(2, 3), keepdims=True)  8.16 us
    squeeze x8, local copies, waits for them, and re-layouts, per_device(): attended = lax.map(attend_block, (grouped, picked, visible))  7.81 us
    broadcast_in_dim x8, local copies, waits for them, and re-layouts, attend_block(): scores = jnp.where(seen[None], scores, -1e+30)  7.31 us
  transfers between devices with their start and end apart: 6, of which 4 were waited for; matrix products, arithmetic and copies ran while one was open for 41% of the time, Pallas kernels for 0%

profile of v1, /device:TPU:0, one launch (start us, length us, event | category | flops | bytes accessed | tf_op | source)
XLA Modules:
  0.0 157.1 jit_solution(17025253862587367967)
XLA Ops:
  7.3 16.7 %all_gather.13 = bf16[2048,64]{0,1:T(8,128)(2,1)S(1)} all-gather(bf16[512,64]{0,1:T(8,128)(2,1)} %param.13), channel_id=1, replica_groups=mesh['dp'=4,'kv'=4,'tp'=2] {'kv'}, dimensions={0}, use_global_device_ids=true | all-gather | bytes 327680 | tf_op jit(solution)/shard_map/all_gather | solution.py:31
  24.0 17.7 %all_gather.12 = bf16[2048,64]{0,1:T(8,128)(2,1)S(1)} all-gather(bf16[512,64]{0,1:T(8,128)(2,1)} %param.12), channel_id=1, replica_groups=mesh['dp'=4,'kv'=4,'tp'=2] {'kv'}, dimensions={0}, use_global_device_ids=true | all-gather | bytes 327680 | tf_op jit(solution)/shard_map/all_gather | solution.py:30
  43.2 1.6 %collective-permute-start = (bf16[512,128]{0,1:T(8,128)(2,1)S(1)}, bf16[512,128]{0,1:T(8,128)(2,1)S(1)}, u32[]{:S(2)}, u32[]{:S(2)}) collective-permute-start(bf16[512,128]{0,1:T(8,128)(2,1)S(1)} %pad_maximum_fusion), channel_id=1, source_target_pairs={{0,2},{2,4},{4,6},{6,0},{1,3},{3,5},{5,7},{7,1},{8,10},{10,12},{12... | collective-permute-start | bytes 393224 | tf_op jit(solution)/shard_map/ppermute | solution.py:19
  45.1 2.6 %compare_and_fusion = pred[8,64,16,64]{1,3,2,0:T(8,128)(4,1)} fusion(s32[8,64]{1,0:T(8,128)S(1)} %iota_add_fusion.1, s32[8,16,64]{2,1,0:T(8,128)S(1)} %iota_add_fusion, pred[8,16]{1,0:T(8,128)(4,1)S(1)} %get-tuple-element.55), kind=kLoop, calls=%fused_computation.20 | loop fusion | flops 1048576 | bytes 559232 | tf_op jit(solution)/shard_map/and | solution.py:52
  47.8 5.9 %collective-permute-done = bf16[512,128]{0,1:T(8,128)(2,1)S(1)} collective-permute-done((bf16[512,128]{0,1:T(8,128)(2,1)S(1)}, bf16[512,128]{0,1:T(8,128)(2,1)S(1)}, u32[]{:S(2)}, u32[]{:S(2)}) %collective-permute-start) | collective-permute-done | bytes 131104 | tf_op jit(solution)/shard_map/ppermute | solution.py:19
  54.4 11.5 %collective-permute-done.1 = bf16[512,128]{0,1:T(8,128)(2,1)S(1)} collective-permute-done((bf16[512,128]{0,1:T(8,128)(2,1)S(1)}, bf16[512,128]{0,1:T(8,128)(2,1)S(1)}, u32[]{:S(2)}, u32[]{:S(2)}) %collective-permute-start.1) | collective-permute-done | bytes 131104 | tf_op jit(solution)/shard_map/ppermute | solution.py:19
  66.1 6.6 %collective-permute-done.2 = bf16[512,128]{0,1:T(8,128)(2,1)S(1)} collective-permute-done((bf16[512,128]{0,1:T(8,128)(2,1)S(1)}, bf16[512,128]{0,1:T(8,128)(2,1)S(1)}, u32[]{:S(2)}, u32[]{:S(2)}) %collective-permute-start.2) | collective-permute-done | bytes 131104 | tf_op jit(solution)/shard_map/ppermute | solution.py:19
  72.9 2.2 %gather_fusion = bf16[128,64,128]{2,1,0:T(8,128)(2,1)} fusion(bf16[32,64,128]{2,1,0:T(8,128)(2,1)S(1)} %bitcast.82, s32[1024]{0:T(1024)S(1)} %pad_clamp_fusion), kind=kCustom, calls=%fused_computation | custom fusion | bytes 4194816 | tf_op jit(solution)/shard_map/jit(_take)/gather | solution.py:44
  75.0 3.3 %broadcast_select_fusion = bf16[8,16,64,128]{3,2,1,0:T(8,128)(2,1)} fusion(bf16[8,16,64,128]{3,2,1,0:T(8,128)(2,1)} %bitcast.83, pred[8,16]{1,0:T(8,128)(4,1)S(1)} %get-tuple-element.56), kind=kLoop, calls=%fused_computation.27 | loop fusion | flops 1048576 | bytes 4194432 | tf_op jit(solution)/shard_map/jit(_take)/select_n | solution.py:44
  78.3 3.7 %convolution_convert_fusion.1 = bf16[512,512]{1,0:T(8,128)(2,1)} fusion(bf16[512,2048]{1,0:T(8,128)(2,1)S(1)} %copy-done, bf16[2048,512]{1,0:T(8,128)(2,1)} %all-gather.3.cloned.1.call-done), kind=kOutput, calls=%fused_computation.28 | convolution fusion | flops 1074003968 | bytes 4718592 | tf_op jit(solution)/shard_map/dot_general | solution.py:33
  82.0 1.6 %reshape.58 = bf16[8,64,8,64]{3,2,1,0:T(8,128)(2,1)S(1)} reshape(bf16[512,512]{1,0:T(8,128)(2,1)} %convolution_convert_fusion.1) | data formatting | bytes 1048576 | tf_op jit(solution)/shard_map/reshape | solution.py:46
  83.6 47.3 %while.10 = (s32[]{:T(128)}, bf16[8,64,8,64]{3,2,1,0:T(8,128)(2,1)}, bf16[8,16,64,128]{3,2,1,0:T(8,128)(2,1)}, pred[8,64,16,64]{1,3,2,0:T(8,128)(4,1)}, bf16[8,64,8,64]{3,2,1,0:T(8,128)(2,1)S(1)}, /*index=5*/s32[]{:T(128)}) while((s32[]{:T(128)}, bf16[8,64,8,64]{3,2,1,0:T(8,128)(2,1)}, bf16[8,16,64,128]{3,2,1,0:T(8,128)(2,1)}, ...), condition=%wide.region_3.4_spmd, body=%wide.region_0.3_spmd.sunk | while | flops 140540928 | bytes 8268369 | solution.py:73
  87.5 1.2 fusion.25
  93.4 1.2 fusion.25
  99.3 1.2 fusion.25
  105.3 1.2 fusion.25
  111.2 1.3 fusion.25
  117.1 1.2 fusion.25
  123.0 1.2 fusion.25
  131.0 1.9 %reshape.59 = bf16[512,512]{1,0:T(8,128)(2,1)S(1)} reshape(bf16[8,64,8,64]{3,2,1,0:T(8,128)(2,1)} %get-tuple-element.32) | data formatting | bytes 1048576 | tf_op jit(solution)/shard_map/reshape | solution.py:74
  132.9 4.2 %convolution_convert_fusion = bf16[512,2048]{1,0:T(8,128)(2,1)} fusion(bf16[512,512]{1,0:T(8,128)(2,1)S(1)} %reshape.59, bf16[512,2048]{1,0:T(8,128)(2,1)} %all-gather.5.cloned.1.call-done), kind=kOutput, calls=%fused_computation.21 | convolution fusion | flops 1074790400 | bytes 4718592 | tf_op jit(solution)/shard_map/dot_general | solution.py:77
  137.1 9.5 %reduce-scatter.2.cloned.1.call-done = bf16[256,2048]{1,0:T(8,128)(2,1)} async-done(((bf16[512,2048]{1,0:T(8,128)(2,1)}), bf16[256,2048]{1,0:T(8,128)(2,1)}) %reduce-scatter.2.cloned.1.call-update) | async-done | bytes 1048592 | tf_op jit(solution)/shard_map/reduce_scatter | solution.py:76
  146.5 1.5 fusion.9
  148.1 2.5 %fusion.11 = bf16[256,2048]{1,0:T(8,128)(2,1)} fusion(bf16[256,2048]{1,0:T(8,128)(2,1)} %reduce-scatter.2.cloned.1.call-done, f32[2048]{0:T(1024)S(1)} %copy-done.2, f32[256]{0:T(256)S(1)} %add_rsqrt_fusion), kind=kLoop, calls=%fused_computation.26 | loop fusion | flops 2097152 | bytes 2106368 | tf_op jit(solution)/shard_map/convert_element_type | solution.py:83
  (94 shorter events, 41.9 us)
Async XLA Ops:
  6.5 35.1 %copy-start = (bf16[512,2048]{1,0:T(8,128)(2,1)S(1)}, bf16[512,2048]{1,0:T(8,128)(2,1)}, u32[]{:S(2)}) copy-start(bf16[512,2048]{1,0:T(8,128)(2,1)} %param.9) | copy-start | bytes 6291460
  6.5 71.8 %all-gather.3.cloned.1.call-start = ((), (), s32[]{:S(2)}) async-start(), calls=%async_computation.1 | async-start | bytes 2621440 | tf_op jit(solution)/shard_map/all_gather | solution.py:29
  7.3 125.6 %all-gather.5.cloned.1.call-start = ((), (), s32[]{:S(2)}) async-start(), calls=%async_computation.2 | async-start | bytes 2621440 | tf_op jit(solution)/shard_map/all_gather | solution.py:75
  42.4 2.4 %copy-start.1 = (s32[8,16]{1,0:T(8,128)S(1)}, s32[8,16]{1,0:T(8,128)}, u32[]{:S(2)}) copy-start(s32[8,16]{1,0:T(8,128)} %param.10) | copy-start | bytes 1540
  43.2 10.4 %collective-permute-start = (bf16[512,128]{0,1:T(8,128)(2,1)S(1)}, bf16[512,128]{0,1:T(8,128)(2,1)S(1)}, u32[]{:S(2)}, u32[]{:S(2)}) collective-permute-start(bf16[512,128]{0,1:T(8,128)(2,1)S(1)} %pad_maximum_fusion), channel_id=1, source_target_pairs={{0,2},{2,4},{4,6},{6,0},{1,3},{3,5},{5,7},{7,1},{8,10},{10,12},{12... | collective-permute-start | bytes 393224 | tf_op jit(solution)/shard_map/ppermute | solution.py:19
  44.8 101.7 %reduce-scatter.2.cloned.1.call-start = ((), (), s32[]{:S(2)}) async-start(), calls=%async_computation.3 | async-start | bytes 3145728 | tf_op jit(solution)/shard_map/reduce_scatter | solution.py:76
  53.6 12.3 %collective-permute-start.1 = (bf16[512,128]{0,1:T(8,128)(2,1)S(1)}, bf16[512,128]{0,1:T(8,128)(2,1)S(1)}, u32[]{:S(2)}, u32[]{:S(2)}) collective-permute-start(bf16[512,128]{0,1:T(8,128)(2,1)S(1)} %collective-permute-done), channel_id=1, source_target_pairs={{0,2},{2,4},{4,6},{6,0},{1,3},{3,5},{5,7},{7,1},{8,10},{10,12},{12... | collective-permute-start | bytes 393224 | tf_op jit(solution)/shard_map/ppermute | solution.py:19
  65.9 6.8 %collective-permute-start.2 = (bf16[512,128]{0,1:T(8,128)(2,1)S(1)}, bf16[512,128]{0,1:T(8,128)(2,1)S(1)}, u32[]{:S(2)}, u32[]{:S(2)}) collective-permute-start(bf16[512,128]{0,1:T(8,128)(2,1)S(1)} %collective-permute-done.1), channel_id=1, source_target_pairs={{0,2},{2,4},{4,6},{6,0},{1,3},{3,5},{5,7},{7,1},{8,10},{10,12},{12... | collective-permute-start | bytes 393224 | tf_op jit(solution)/shard_map/ppermute | solution.py:19
  137.1 11.0 %copy-start.2 = (f32[2048]{0:T(1024)S(1)}, f32[2048]{0:T(1024)}, u32[]{:S(2)}) copy-start(f32[2048]{0:T(1024)} %param.15) | copy-start | bytes 24580
Sparse Core Ops, SparseCore 0:
  8.9 59.7 all-gather.2
  70.3 44.3 all-gather.4
  137.2 9.2 reduce-scatter.1
